TPU v7x, 256 devices: a whole 4x4x8 slice. The times are simulated.
256 devices in a mesh: sp: 64 (over z, y, core), tp: 4 (over x).
Axes of the slice: x: 4, y: 4, z: 8, core: 2. Of those that a mesh axis runs over, the one named last changes fastest.
Arguments:
- resid: bfloat16 [12288, 2048], P(('sp', 'tp')), may hold values from -6 to 6
- query_a: bfloat16 [12288, 1024], P('sp', 'tp'), may hold values from -12 to 12
- key_a: bfloat16 [12288, 1024], P('sp', 'tp'), may hold values from -12 to 12
- value_a: bfloat16 [12288, 1024], P('sp', 'tp'), may hold values from -6 to 6
- query_b: bfloat16 [12288, 128], P('sp', 'tp'), may hold values from -12 to 12
- key_b: bfloat16 [12288, 128], P('sp', 'tp'), may hold values from -12 to 12
- value_b: bfloat16 [12288, 128], P('sp', 'tp'), may hold values from -6 to 6
- out_a: bfloat16 [1024, 2048], P('tp'), may hold values from -0.1875 to 0.1875
- out_b: bfloat16 [128, 2048], P('tp'), may hold values from -0.5 to 0.5
- attn_gain: float32 [2048], replicated, may hold values from 0.1 to 1.9
- mlp_gain: float32 [2048], replicated, may hold values from 0.1 to 1.9
- gate_weight: bfloat16 [2048, 5632], P('sp', 'tp'), may hold values from -0.125 to 0.125
- up_weight: bfloat16 [2048, 5632], P('sp', 'tp'), may hold values from -0.125 to 0.125
- down_weight: bfloat16 [5632, 2048], P('tp', 'sp'), may hold values from -0.078125 to 0.078125
Outputs:
- result: bfloat16 [12288, 2048], P(('sp', 'tp'))
All inputs are finite; a program needn't handle non-finite values.
Results may differ from a plain program's by a relative error of at most 0.014.
Values may be sent and summed in bfloat16 or wider, within the bound.
A program may use at most 128 MiB of HBM per device.

v0:
```python
import jax
import jax.numpy as jnp
from jax import lax
from jax.sharding import PartitionSpec as P

HEAD_A = 256
HEAD_B = 32


epsilon = 1e-06


def sent_together(arrays, axis, dim, along):
    ends, at = ([], 0)
    for a in arrays[:-1]:
        at += a.shape[along]
        ends.append(at)
    both = jnp.concatenate(arrays, axis=along)
    return tuple(jnp.split(lax.all_gather(both, axis, axis=dim, tiled=True), ends, axis=along))


def cut_along(x, dim, devices):
    shape = x.shape
    pieces = x.reshape(*shape[:dim], devices, shape[dim] // devices, *shape[dim + 1 :])
    return jnp.moveaxis(pieces, dim, 0)


def summed_on_arrival(x, axis, dim):
    devices = lax.axis_size(axis)
    pieces = lax.all_to_all(cut_along(x, dim, devices), axis, 0, 0, tiled=True)
    return jnp.sum(pieces.astype(jnp.float32), axis=0)


def turned_gather(arrays, axis, dims):
    turned = [jnp.moveaxis(a, dim, 0) for a, dim in zip(arrays, dims)]
    both = jnp.concatenate([t.reshape(len(t), -1) for t in turned], axis=1)
    result, at, gathered = (lax.all_gather(both, axis, axis=0, tiled=True), 0, [])
    for t, dim in zip(turned, dims):
        section = result[:, at : at + t[0].size].reshape(-1, *t.shape[1:])
        gathered.append(jnp.moveaxis(section, 0, dim))
        at += t[0].size
    return tuple(gathered)


def joined_along(pieces, dim):
    pieces = jnp.moveaxis(pieces, 0, dim)
    shape = pieces.shape
    return pieces.reshape(*shape[:dim], shape[dim] * shape[dim + 1], *shape[dim + 2 :])


def copy_for_each(x, axis):
    copies = jnp.broadcast_to(x, (lax.axis_size(axis), *x.shape))
    return lax.all_to_all(copies, axis, split_axis=0, concat_axis=0, tiled=True)


def gather_directly(x, axis, dim):
    return joined_along(copy_for_each(x, axis), dim)


def stick_weights(queries, key_rows, anchor, factor):
    amount = queries.shape[0]
    heads = queries.shape[1]
    length = key_rows.shape[0]
    block_len = min(512, length)
    sub_len = min(128, block_len)
    block_count = length // block_len
    sub_count = block_len // sub_len
    key_tiles = key_rows.reshape(block_count, block_len, heads, key_rows.shape[2])
    inner_mask = (jnp.arange(sub_len)[:, None] > jnp.arange(sub_len)[None, :]).astype(jnp.float32)
    outer_mask = (jnp.arange(sub_count)[:, None] > jnp.arange(sub_count)[None, :]).astype(
        jnp.float32
    )
    query_pos = anchor + jnp.arange(amount, dtype=jnp.int32)

    def step(suffix, inputs):
        key_tile, block_id = inputs
        scores = (
            jnp.einsum("qhd,khd->qhk", queries, key_tile, preferred_element_type=jnp.float32)
            * factor
        )
        key_pos = block_id * block_len + jnp.arange(block_len, dtype=jnp.int32)
        causal = (key_pos[None, :] < query_pos[:, None])[:, None, :]
        log_keep = jnp.where(causal, jax.nn.log_sigmoid(-scores), 0.0)
        split_keep = log_keep.reshape(amount, heads, sub_count, sub_len)
        within = jnp.einsum("qhcj,js->qhcs", split_keep, inner_mask)
        sub_totals = jnp.sum(split_keep, axis=-1)
        after_sub = jnp.einsum("qhc,cd->qhd", sub_totals, outer_mask)
        later_sum = (within + after_sub[..., None]).reshape(amount, heads, block_len) + suffix[
            :, :, None
        ]
        log_weight = jnp.where(causal, scores + log_keep + later_sum, -1e30)
        weight = jnp.exp(log_weight).astype(jnp.bfloat16)
        return (suffix + jnp.sum(sub_totals, axis=-1), weight)

    start_sum = jnp.zeros((amount, heads), jnp.float32)
    ignored, stacked = lax.scan(
        step, start_sum, (key_tiles, jnp.arange(block_count, dtype=jnp.int32)), reverse=True
    )
    return jnp.moveaxis(stacked, 0, 2).reshape(amount, heads, length)


def round_trip(values):
    return lax.optimization_barrier(values.astype(jnp.bfloat16)).astype(jnp.float32)


def row_norm(values, gain_row):
    return (
        values * lax.rsqrt(jnp.mean(values * values, axis=-1, keepdims=True) + epsilon) * gain_row
    )


def body(
    resid,
    query_a,
    key_a,
    value_a,
    query_b,
    key_b,
    value_b,
    out_a,
    out_b,
    attn_gain,
    mlp_gain,
    gate_weight,
    up_weight,
    down_weight,
):
    rows_here = query_a.shape[0]
    heads_a = out_a.shape[0] // HEAD_A
    heads_b = out_b.shape[0] // HEAD_B
    keys_a, keys_b = sent_together((key_a, key_b), "sp", 0, 1)
    anchor = lax.axis_index("sp") * rows_here
    weights_a = stick_weights(
        query_a.reshape(rows_here, heads_a, HEAD_A),
        keys_a.reshape(-1, heads_a, HEAD_A),
        anchor,
        HEAD_A ** (-0.5),
    )
    weights_b = stick_weights(
        query_b.reshape(rows_here, heads_b, HEAD_B),
        keys_b.reshape(-1, heads_b, HEAD_B),
        anchor,
        HEAD_B ** (-0.5),
    )
    pieces = sent_together((value_a, value_b), "sp", 0, 1)
    amount = pieces[0].shape[0]
    total_a = jnp.einsum(
        "qhk,khd->qhd",
        weights_a,
        pieces[0].reshape(amount, heads_a, HEAD_A),
        preferred_element_type=jnp.float32,
    )
    total_b = jnp.einsum(
        "qhk,khd->qhd",
        weights_b,
        pieces[1].reshape(amount, heads_b, HEAD_B),
        preferred_element_type=jnp.float32,
    )
    attended_a = total_a.astype(jnp.bfloat16).reshape(rows_here, heads_a * HEAD_A)
    attended_b = total_b.astype(jnp.bfloat16).reshape(rows_here, heads_b * HEAD_B)
    term = jnp.dot(attended_a, out_a, preferred_element_type=jnp.float32)
    term = term + jnp.dot(attended_b, out_b, preferred_element_type=jnp.float32)
    projected = summed_on_arrival(round_trip(term).astype(jnp.bfloat16), "tp", 0)
    gate_whole, up_whole, down_whole = turned_gather(
        (gate_weight, up_weight, down_weight), "sp", (0, 0, 1)
    )
    middle = (resid.astype(jnp.float32) + row_norm(projected, attn_gain)).astype(jnp.bfloat16)
    middle_f = middle.astype(jnp.float32)
    normed_rows = row_norm(middle_f, mlp_gain).astype(jnp.bfloat16)
    channel_input = gather_directly(normed_rows, "tp", 0)
    gate_sums = jnp.dot(channel_input, gate_whole, preferred_element_type=jnp.float32)
    up_sums = jnp.dot(channel_input, up_whole, preferred_element_type=jnp.float32)
    hidden = (jax.nn.silu(gate_sums) * up_sums).astype(jnp.bfloat16)
    mixer_sum = summed_on_arrival(
        round_trip(jnp.dot(hidden, down_whole, preferred_element_type=jnp.float32)).astype(
            jnp.bfloat16
        ),
        "tp",
        0,
    )
    return (middle_f + mixer_sum).astype(jnp.bfloat16)


def solution(mesh):
    return jax.shard_map(
        body,
        mesh=mesh,
        in_specs=(
            P(("sp", "tp"), None),
            P("sp", "tp"),
            P("sp", "tp"),
            P("sp", "tp"),
            P("sp", "tp"),
            P("sp", "tp"),
            P("sp", "tp"),
            P("tp", None),
            P("tp", None),
            P(),
            P(),
            P("sp", "tp"),
            P("sp", "tp"),
            P("tp", "sp"),
        ),
        out_specs=P(("sp", "tp"), None),
        check_vma=False,
    )
```

profile of v0, /device:TPU:1, one launch (start us, length us, event | category | flops | bytes accessed | tf_op | source)
XLA Modules:
  0.0 428.2 jit_solution(8940086735355853781)
XLA Ops:
  7.5 1.6 pad_maximum_fusion.1
  9.9 1.6 pad_maximum_fusion.2
  11.6 1.7 pad_maximum_fusion
  13.4 85.1 %all-gather.6.cloned.1.call-done = bf16[12288,288]{1,0:T(8,128)(2,1)} async-done(((bf16[192,288]{1,0:T(8,128)(2,1)}), bf16[12288,288]{1,0:T(8,128)(2,1)}) %all-gather.6.cloned.1.call-update) | async-done | bytes 7077904 | tf_op jit(solution)/shard_map/all_gather | solution.py:19
  98.5 6.5 %split.16 = bf16[12288,256]{1,0:T(8,128)(2,1)} slice(bf16[12288,288]{1,0:T(8,128)(2,1)} %all-gather.6.cloned.1.call-done), slice={[0:12288], [0:256]} | slice | bytes 12582912 | tf_op jit(solution)/shard_map/split | solution.py:19
  104.9 2.7 broadcast.243.clone
  107.7 123.8 %while.34 = (s32[]{:T(128)}, f32[192,1]{0,1:T(1,128)S(1)}, bf16[24,192,1,512]{3,1,2,0:T(8,128)(2,1)}, s32[24]{0:T(128)S(1)}, bf16[24,512,1,256]{3,1,2,0:T(8,128)...) while((s32[]{:T(128)}, f32[192,1]{0,1:T(1,128)S(1)}, ...), condition=%wide.region_3.4_spmd.clone, body=%wide.region_0.3_spmd.clone.sunk | while | flops 78190752 | bytes 5691319 | solution.py:96
  108.9 1.5 compare_select_fusion.8
  165.6 1.5 compare_select_fusion.8
  175.9 1.6 compare_select_fusion.8
  201.8 1.5 compare_select_fusion.8
  231.5 5.8 %copy.35 = bf16[24,8,24,512]{3,1,2,0:T(8,128)(2,1)} copy(bf16[24,8,24,512]{3,1,0,2:T(8,128)(2,1)} %bitcast.134) | data formatting | bytes 9437184
  237.3 3.2 split.19
  240.5 3.1 copy.31
  243.7 2.6 broadcast.243.clone.1
  246.3 101.0 %while.35 = (s32[]{:T(128)}, f32[192,1]{0,1:T(1,128)S(1)}, bf16[24,192,1,512]{3,1,2,0:T(8,128)(2,1)}, s32[24]{0:T(128)S(1)}, bf16[24,512,1,32]{1,3,2,0:T(8,128)(...) while((s32[]{:T(128)}, f32[192,1]{0,1:T(1,128)S(1)}, ...), condition=%wide.region_7.8_spmd.clone, body=%wide.region_4.7_spmd.clone.sunk | while | flops 34150564 | bytes 5380279 | solution.py:96
  347.3 5.2 %copy.36 = bf16[24,8,24,512]{3,1,2,0:T(8,128)(2,1)} copy(bf16[24,8,24,512]{3,1,0,2:T(8,128)(2,1)} %bitcast.132) | data formatting | bytes 9437184
  352.5 6.4 %fusion.73 = f32[192,2048]{1,0:T(8,128)S(1)} fusion(bf16[256,2048]{1,0:T(8,128)(2,1)S(1)} %copy-done, bf16[192,12288]{1,0:T(8,128)(2,1)} %bitcast.137, bf16[12288,288]{1,0:T(8,128)(2,1)} %all-gather.4.cloned.1.call-done), kind=kOutput, calls=%fused_computation.77 | convolution fusion | flops 1409335296 | bytes 13631488 | tf_op jit(solution)/shard_map/dot_general | solution.py:161
  358.9 5.6 %fusion.63 = bf16[192,2048]{1,0:T(8,128)(2,1)S(1)} fusion(f32[192,2048]{1,0:T(8,128)S(1)} %fusion.73, bf16[32,2048]{1,0:T(8,128)(2,1)S(1)} %copy-done.1, bf16[192,12288]{1,0:T(8,128)(2,1)} %bitcast.133, bf16[12288,288]{1,0:T(8,128)(2,1)} %all-gather.4.cloned.1.call-done), kind=kOutput, calls=%fused_computation.72 | convolution fusion | flops 176953344 | bytes 10354688 | tf_op jit(solution)/shard_map/dot_general | solution.py:162
  364.5 15.7 %all_to_all.15 = bf16[4,48,2048]{2,1,0:T(8,128)(2,1)S(1)} all-to-all(bf16[4,48,2048]{2,1,0:T(8,128)(2,1)S(1)} %bitcast.138), channel_id=1, replica_groups=mesh['sp'=64,'tp'=4] {'tp'}, dimensions={0} | all-to-all | bytes 1572864 | tf_op jit(solution)/shard_map/all_to_all | solution.py:30
  381.9 13.6 %all_to_all.16 = bf16[4,48,2048]{2,1,0:T(8,128)(2,1)S(1)} all-to-all(bf16[4,48,2048]{2,1,0:T(8,128)(2,1)S(1)} %broadcast_in_dim.65), channel_id=1, replica_groups=mesh['sp'=64,'tp'=4] {'tp'}, dimensions={0} | all-to-all | bytes 1572864 | tf_op jit(solution)/shard_map/all_to_all | solution.py:53
  395.5 5.0 %fusion.50 = f32[192,1408]{1,0:T(8,128)} fusion(bf16[192,2048]{1,0:T(8,128)(2,1)S(1)} %bitcast.139, bf16[2048,4224]{1,0:T(8,128)(2,1)} %all-gather.8.cloned.1.call-done), kind=kOutput, calls=%fused_computation.64 | convolution fusion | flops 1107296256 | bytes 7634944 | tf_op jit(solution)/shard_map/dot_general | solution.py:171
  400.5 7.9 %fusion.60 = bf16[192,2048]{1,0:T(8,128)(2,1)S(1)} fusion(bf16[2048,4224]{1,0:T(8,128)(2,1)} %all-gather.8.cloned.1.call-done, bf16[192,2048]{1,0:T(8,128)(2,1)S(1)} %bitcast.140, f32[192,1408]{1,0:T(8,128)} %fusion.50), kind=kOutput, calls=%fused_computation.71 | convolution fusion | flops 2216607744 | bytes 14188544 | tf_op jit(solution)/shard_map/dot_general | solution.py:175
  408.4 12.4 %all_to_all.17 = bf16[4,48,2048]{2,1,0:T(8,128)(2,1)S(1)} all-to-all(bf16[4,48,2048]{2,1,0:T(8,128)(2,1)S(1)} %bitcast.141), channel_id=1, replica_groups=mesh['sp'=64,'tp'=4] {'tp'}, dimensions={0} | all-to-all | bytes 1572864 | tf_op jit(solution)/shard_map/all_to_all | solution.py:30
  (607 shorter events, 189.0 us)
Async XLA Ops:
  6.5 346.0 %copy-start = (bf16[256,2048]{1,0:T(8,128)(2,1)S(1)}, bf16[256,2048]{1,0:T(8,128)(2,1)}, u32[]{:S(2)}) copy-start(bf16[256,2048]{1,0:T(8,128)(2,1)} %param.25) | copy-start | bytes 3145732
  6.5 91.9 %all-gather.6.cloned.1.call-start = ((), (), s32[]{:S(2)}) async-start(), calls=%async_computation.4 | async-start | bytes 9584640 | tf_op jit(solution)/shard_map/all_gather | solution.py:19
  9.1 343.4 %all-gather.4.cloned.1.call-start = ((), (), s32[]{:S(2)}) async-start(), calls=%async_computation.3 | async-start | bytes 9584640 | tf_op jit(solution)/shard_map/all_gather | solution.py:19
  11.6 383.9 %all-gather.8.cloned.1.call-start = ((), (), s32[]{:S(2)}) async-start(), calls=%async_computation.5 | async-start | bytes 17571840 | tf_op jit(solution)/shard_map/all_gather | solution.py:37
  104.9 2.7 copy-start.4
  240.5 5.8 %copy-start.5 = (bf16[192,32]{0,1:T(8,128)(2,1)S(1)}, bf16[192,32]{0,1:T(8,128)(2,1)}, u32[]{:S(2)}) copy-start(bf16[192,32]{0,1:T(8,128)(2,1)} %param.22) | copy-start | bytes 36868
  352.5 6.4 %copy-start.1 = (bf16[32,2048]{1,0:T(8,128)(2,1)S(1)}, bf16[32,2048]{1,0:T(8,128)(2,1)}, u32[]{:S(2)}) copy-start(bf16[32,2048]{1,0:T(8,128)(2,1)} %param.26) | copy-start | bytes 393220
  358.9 21.6 %copy-start.2 = (f32[2048]{0:T(1024)S(1)}, f32[2048]{0:T(1024)}, u32[]{:S(2)}) copy-start(f32[2048]{0:T(1024)} %param.27) | copy-start | bytes 24580
  358.9 22.8 %copy-start.3 = (f32[2048]{0:T(1024)S(1)}, f32[2048]{0:T(1024)}, u32[]{:S(2)}) copy-start(f32[2048]{0:T(1024)} %param.28) | copy-start | bytes 24580
Sparse Core Ops, SparseCore 0:
  10.1 88.3 all-gather.5
  101.2 81.2 all-gather.3
  185.3 97.7 all-gather.7
where the time goes:
time: 431 us; the launch traced here: 428 us
  matrix products  94.9 us (22%)
  local copies, waits for them, and re-layouts  85.5 us (20%)
  waiting for transfers between devices  85.2 us (20%)
  other arithmetic  73.6 us (17%)
  blocking collectives  41.7 us (10%)
  loops' own time  34.1 us (8%)
  between operations  13.2 us (3%)
    all_gather x2, waiting for transfers between devices, sent_together(): lax.all_gather(both, axis, axis=dim, tiled=True)  85.1 us
    dot_general x48, matrix products, step(): jnp.einsum('qhd,khd->qhk', queries, key_tile, preferred_element_type=jnp....  51.1 us
    dynamic_update_slice x48, other arithmetic, stick_weights(): lax.scan(step, start_sum, (key_tiles, jnp.arange(block_count, dtype=jnp.i...  50 us
    another operation x2, loops' own time, stick_weights(): lax.scan(step, start_sum, (key_tiles, jnp.arange(block_count, dtype=jnp.i...  34.1 us
    all_to_all x2, blocking collectives, summed_on_arrival(): pieces = lax.all_to_all(cut_along(x, dim, devices), axis, 0, 0, tiled=True)  28.1 us
    dynamic_slice x48, local copies, waits for them, and re-layouts, stick_weights(): lax.scan(step, start_sum, (key_tiles, jnp.arange(block_count, dtype=jnp.i...  27.9 us
    unnamed x17, local copies, waits for them, and re-layouts  15.9 us
    reduce_sum x48, other arithmetic, step(): sub_totals = jnp.sum(split_keep, axis=-1)  15.2 us
  transfers between devices with their start and end apart: 3, of which 1 were waited for; matrix products, arithmetic and copies ran while one was open for 56% of the time, Pallas kernels for 0%

commit v1 on v0

v1 whole, which is shorter than its diff:
```python
import functools
import math

import jax
import jax.numpy as jnp
from jax import lax
from jax.experimental import pallas as pl
from jax.experimental.pallas import tpu as pltpu
from jax.sharding import PartitionSpec as P

MESH = pl.DeviceIdType.MESH
HEAD_A = 256
HEAD_B = 32
PACK = 640
TILE = 512
SUB = 256
CORES = 2
NY = 4

epsilon = 1e-06


def cut_along(x, dim, devices):
    shape = x.shape
    pieces = x.reshape(*shape[:dim], devices, shape[dim] // devices, *shape[dim + 1 :])
    return jnp.moveaxis(pieces, dim, 0)


def summed_on_arrival(x, axis, dim):
    devices = lax.axis_size(axis)
    pieces = lax.all_to_all(cut_along(x, dim, devices), axis, 0, 0, tiled=True)
    return jnp.sum(pieces.astype(jnp.float32), axis=0)


def turned_gather(arrays, axis, dims):
    turned = [jnp.moveaxis(a, dim, 0) for a, dim in zip(arrays, dims)]
    both = jnp.concatenate([t.reshape(len(t), -1) for t in turned], axis=1)
    result, at, gathered = (lax.all_gather(both, axis, axis=0, tiled=True), 0, [])
    for t, dim in zip(turned, dims):
        section = result[:, at : at + t[0].size].reshape(-1, *t.shape[1:])
        gathered.append(jnp.moveaxis(section, 0, dim))
        at += t[0].size
    return tuple(gathered)


def joined_along(pieces, dim):
    pieces = jnp.moveaxis(pieces, 0, dim)
    shape = pieces.shape
    return pieces.reshape(*shape[:dim], shape[dim] * shape[dim + 1], *shape[dim + 2 :])


def copy_for_each(x, axis):
    copies = jnp.broadcast_to(x, (lax.axis_size(axis), *x.shape))
    return lax.all_to_all(copies, axis, split_axis=0, concat_axis=0, tiled=True)


def gather_directly(x, axis, dim):
    return joined_along(copy_for_each(x, axis), dim)


def gather_kernel(nz, ny, cuts, x_ref, o_ref, send_sem, recv_sem, pair_send, pair_recv, own_sem):
    rows = x_ref.shape[0]
    me = lax.axis_index("sp")
    c = lax.rem(me, CORES)
    y = lax.rem(me // CORES, ny)
    z = me // (CORES * ny)

    def device(zz, yy, cc):
        return (zz * ny + yy) * CORES + cc

    partner = device(z, y, 1 - c)
    around = {
        ("y", 1): device(z, lax.rem(y + 1, ny), c),
        ("y", -1): device(z, lax.rem(y + ny - 1, ny), c),
        ("z", 1): device(lax.rem(z + 1, nz), y, c),
        ("z", -1): device(lax.rem(z + nz - 1, nz), y, c),
    }
    barrier = pltpu.get_barrier_semaphore()
    for other in (partner, *around.values()):
        pl.semaphore_signal(barrier, inc=1, device_id={"sp": other}, device_id_type=MESH)
    pl.semaphore_wait(barrier, 5)

    size = {"y": ny, "z": nz}
    colours = []
    at = 0
    for n, (first, second, way) in enumerate(
        (("y", "z", 1), ("y", "z", -1), ("z", "y", 1), ("z", "y", -1))
    ):
        colours.append((n, first, second, way, at, cuts[n]))
        at += cuts[n]

    def block(ref_rows_of, start, count):
        return o_ref.at[pl.ds(pl.multiple_of(ref_rows_of + start, 8), count)]

    def base_of(zz, yy):
        return device(zz, yy, c) * rows

    own = base_of(z, y)
    own_copy = pltpu.make_async_copy(x_ref, o_ref.at[pl.ds(pl.multiple_of(own, 8), rows)], own_sem)
    own_copy.start()
    pltpu.make_async_remote_copy(
        src_ref=x_ref,
        dst_ref=o_ref.at[pl.ds(pl.multiple_of(own, 8), rows)],
        send_sem=pair_send,
        recv_sem=pair_recv,
        device_id={"sp": partner},
        device_id_type=MESH,
    ).start()

    def send(src, dst, n, index, target):
        pltpu.make_async_remote_copy(
            src_ref=src,
            dst_ref=dst,
            send_sem=send_sem.at[n],
            recv_sem=recv_sem.at[n, index],
            device_id={"sp": target},
            device_id_type=MESH,
        ).start()

    for n, first, second, way, start, count in colours:
        src = x_ref.at[pl.ds(start, count)]
        dst = block(own, start, count)
        send(src, dst, n, 0, around[first, way])
        send(src, dst, n, size[first] - 1, around[second, way])

    def round_of(r, carry):
        for n, first, second, way, start, count in colours:
            na, nb = size[first], size[second]
            early = r < na - 1
            late = r - (na - 1)
            k = jnp.where(early, r + 1, lax.rem(late + na, na))
            m = jnp.where(early, 0, (late + na) // na)
            if first == "y":
                zz = lax.rem(z - way * m + nz, nz)
                yy = lax.rem(y - way * k + ny, ny)
            else:
                zz = lax.rem(z - way * k + nz, nz)
                yy = lax.rem(y - way * m + ny, ny)
            piece = block(base_of(zz, yy), start, count)
            pltpu.make_async_remote_copy(
                src_ref=piece,
                dst_ref=piece,
                send_sem=send_sem.at[n],
                recv_sem=recv_sem.at[n, r],
                device_id={"sp": partner},
                device_id_type=MESH,
            ).wait_recv()

            @pl.when(r < na - 2)
            def _():
                send(piece, piece, n, r + 1, around[first, way])

            @pl.when(early)
            def _():
                send(piece, piece, n, na + r, around[second, way])

            @pl.when(jnp.logical_and(r >= na - 1, r < (na - 1) + (nb - 2) * na))
            def _():
                send(piece, piece, n, r + na, around[second, way])

            pltpu.make_async_remote_copy(
                src_ref=piece,
                dst_ref=piece,
                send_sem=pair_send,
                recv_sem=pair_recv,
                device_id={"sp": partner},
                device_id_type=MESH,
            ).start()
        return carry

    lax.fori_loop(0, nz * ny - 1, round_of, 0)

    def drained(sem, count):
        part = o_ref.at[pl.ds(0, count)]
        pltpu.make_async_copy(part, part, sem).wait()

    own_copy.wait()
    for n, first, second, way, start, count in colours:
        drained(send_sem.at[n], (nz * ny - 1) * count)
    drained(pair_send, nz * ny * rows)
    drained(pair_recv, nz * ny * rows)


def gathered_rows(packed, nz, ny, cuts):
    rows = packed.shape[0]
    return pl.pallas_call(
        functools.partial(gather_kernel, nz, ny, cuts),
        name="gather_rows",
        out_shape=jax.ShapeDtypeStruct((nz * ny * CORES * rows, packed.shape[1]), packed.dtype),
        in_specs=[pl.BlockSpec(memory_space=pltpu.VMEM)],
        out_specs=pl.BlockSpec(memory_space=pl.ANY),
        scratch_shapes=[
            pltpu.SemaphoreType.DMA((4,)),
            pltpu.SemaphoreType.DMA((4, nz * ny - 1)),
            pltpu.SemaphoreType.DMA,
            pltpu.SemaphoreType.DMA,
            pltpu.SemaphoreType.DMA,
        ],
        compiler_params=pltpu.CompilerParams(
            collective_id=0, has_side_effects=True, vmem_limit_bytes=8 * 1024 * 1024
        ),
        cost_estimate=pl.CostEstimate(flops=10**10, bytes_accessed=10**7, transcendentals=0),
    )(packed)


def attention_kernel(
    tiles, tile, anchor_ref, qa_ref, qb_ref, kv_ref, outa_ref, outb_ref, suffix, acca, accb, below
):
    step = pl.program_id(0)
    rows = qa_ref.shape[0]
    anchor = anchor_ref[0]
    start = (tiles - 1 - step) * tile
    nt = (((1,), (1,)), ((), ()))

    @pl.when(step == 0)
    def _():
        suffix[...] = jnp.zeros_like(suffix)
        acca[...] = jnp.zeros_like(acca)
        accb[...] = jnp.zeros_like(accb)
        j = lax.broadcasted_iota(jnp.int32, (SUB, SUB), 0)
        s = lax.broadcasted_iota(jnp.int32, (SUB, SUB), 1)
        below[...] = (j > s).astype(jnp.bfloat16)

    def work(masked):
        for part in reversed(range(tile // SUB)):
            span = pl.ds(part * SUB, SUB)
            if masked:
                key_pos = start + part * SUB + lax.broadcasted_iota(jnp.int32, (rows, SUB), 1)
                query_pos = anchor + lax.broadcasted_iota(jnp.int32, (rows, SUB), 0)
                causal = key_pos < query_pos
            for head, (q_ref, acc, first, width, value, size) in enumerate(
                (
                    (qa_ref, acca, 0, HEAD_A, HEAD_A, HEAD_A),
                    (qb_ref, accb, 2 * HEAD_A, 128, 2 * HEAD_A, HEAD_B),
                )
            ):
                scale = size**-0.5 * math.log2(math.e)
                u = (
                    lax.dot_general(
                        q_ref[...],
                        kv_ref[span, pl.ds(first, width)],
                        nt,
                        preferred_element_type=jnp.float32,
                    )
                    * scale
                )
                soft = jnp.maximum(u, jnp.log2(1.0 + jnp.exp2(jnp.minimum(u, 126.0))))
                if masked:
                    soft = jnp.where(causal, soft, 0.0)
                later = jnp.dot(
                    soft.astype(jnp.bfloat16), below[...], preferred_element_type=jnp.float32
                )
                power = (u - soft) - (later + suffix[head])
                if masked:
                    power = jnp.where(causal, power, -1e30)
                weight = jnp.exp2(power).astype(jnp.bfloat16)
                suffix[head] += jnp.sum(soft, axis=1, keepdims=True)
                acc[...] += jnp.dot(
                    weight,
                    kv_ref[span, pl.ds(value, width)],
                    preferred_element_type=jnp.float32,
                )

    @pl.when(jnp.logical_and(start + tile > anchor, start < anchor + rows))
    def _():
        work(True)

    @pl.when(start + tile <= anchor)
    def _():
        work(False)

    @pl.when(step == tiles - 1)
    def _():
        outa_ref[...] = acca[...].astype(outa_ref.dtype)
        outb_ref[...] = accb[...].astype(outb_ref.dtype)


def attended(anchor, query_a, query_b, kv, tile=TILE):
    rows = query_a.shape[0]
    length = kv.shape[0]
    tiles = length // tile
    return pl.pallas_call(
        functools.partial(attention_kernel, tiles, tile),
        name="stick_attention",
        grid_spec=pltpu.PrefetchScalarGridSpec(
            num_scalar_prefetch=1,
            grid=(tiles,),
            in_specs=[
                pl.BlockSpec((rows, HEAD_A), lambda i, a: (0, 0)),
                pl.BlockSpec((rows, 128), lambda i, a: (0, 0)),
                pl.BlockSpec((tile, PACK), lambda i, a: (tiles - 1 - i, 0)),
            ],
            out_specs=[
                pl.BlockSpec((rows, HEAD_A), lambda i, a: (0, 0)),
                pl.BlockSpec((rows, 128), lambda i, a: (0, 0)),
            ],
            scratch_shapes=[
                pltpu.VMEM((2, rows, 1), jnp.float32),
                pltpu.VMEM((rows, HEAD_A), jnp.float32),
                pltpu.VMEM((rows, 128), jnp.float32),
                pltpu.VMEM((SUB, SUB), jnp.bfloat16),
            ],
        ),
        out_shape=[
            jax.ShapeDtypeStruct((rows, HEAD_A), jnp.bfloat16),
            jax.ShapeDtypeStruct((rows, 128), jnp.bfloat16),
        ],
        compiler_params=pltpu.CompilerParams(
            dimension_semantics=("arbitrary",), vmem_limit_bytes=32 * 1024 * 1024
        ),
        cost_estimate=pl.CostEstimate(
            flops=12 * rows * length * HEAD_A,
            bytes_accessed=length * PACK * 2,
            transcendentals=6 * rows * length,
        ),
    )(anchor, query_a, query_b, kv)


def round_trip(values):
    return lax.optimization_barrier(values.astype(jnp.bfloat16)).astype(jnp.float32)


def row_norm(values, gain_row):
    return (
        values * lax.rsqrt(jnp.mean(values * values, axis=-1, keepdims=True) + epsilon) * gain_row
    )


def body(
    resid,
    query_a,
    key_a,
    value_a,
    query_b,
    key_b,
    value_b,
    out_a,
    out_b,
    attn_gain,
    mlp_gain,
    gate_weight,
    up_weight,
    down_weight,
):
    rows_here = query_a.shape[0]
    chips = lax.axis_size("sp") // CORES
    gate_whole, up_whole, down_whole = turned_gather(
        (gate_weight, up_weight, down_weight), "sp", (0, 0, 1)
    )
    spare = jnp.zeros((rows_here, PACK - 2 * HEAD_A - 2 * HEAD_B), jnp.bfloat16)
    packed = jnp.concatenate([key_a, value_a, key_b, value_b, spare], axis=1)
    kv = gathered_rows(packed, chips // NY, NY, (40, 40, 56, 56))
    anchor = (lax.axis_index("sp") * rows_here).astype(jnp.int32).reshape(1)
    query_b = jnp.pad(query_b, ((0, 0), (0, 128 - HEAD_B)))
    attended_a, wide_b = attended(anchor, query_a, query_b, kv)
    attended_b = wide_b[:, HEAD_B : 2 * HEAD_B]
    term = jnp.dot(attended_a, out_a, preferred_element_type=jnp.float32)
    term = term + jnp.dot(attended_b, out_b, preferred_element_type=jnp.float32)
    projected = summed_on_arrival(round_trip(term).astype(jnp.bfloat16), "tp", 0)
    middle = (resid.astype(jnp.float32) + row_norm(projected, attn_gain)).astype(jnp.bfloat16)
    middle_f = middle.astype(jnp.float32)
    normed_rows = row_norm(middle_f, mlp_gain).astype(jnp.bfloat16)
    channel_input = gather_directly(normed_rows, "tp", 0)
    gate_sums = jnp.dot(channel_input, gate_whole, preferred_element_type=jnp.float32)
    up_sums = jnp.dot(channel_input, up_whole, preferred_element_type=jnp.float32)
    hidden = (jax.nn.silu(gate_sums) * up_sums).astype(jnp.bfloat16)
    mixer_sum = summed_on_arrival(
        round_trip(jnp.dot(hidden, down_whole, preferred_element_type=jnp.float32)).astype(
            jnp.bfloat16
        ),
        "tp",
        0,
    )
    return (middle_f + mixer_sum).astype(jnp.bfloat16)


def solution(mesh):
    return jax.shard_map(
        body,
        mesh=mesh,
        in_specs=(
            P(("sp", "tp"), None),
            P("sp", "tp"),
            P("sp", "tp"),
            P("sp", "tp"),
            P("sp", "tp"),
            P("sp", "tp"),
            P("sp", "tp"),
            P("tp", None),
            P("tp", None),
            P(),
            P(),
            P("sp", "tp"),
            P("sp", "tp"),
            P("tp", "sp"),
        ),
        out_specs=P(("sp", "tp"), None),
        check_vma=False,
    )
```

time: 431 us -> 183 us (0.42)
  the two profiles are of different devices: /device:TPU:1 before, /device:TPU:248 now
where the time goes in v1:
time: 183 us
  Pallas kernels  103 us (56%)
  blocking collectives  44.4 us (24%)
  matrix products  13.7 us (7%)
  between operations  13.5 us (7%)
  local copies, waits for them, and re-layouts  4.34 us (2%)
  other arithmetic  3.28 us (2%)
    pallas_call x1, Pallas kernels, gathered_rows(): pl.pallas_call(functools.partial(gather_kernel, nz, ny, cuts), name='gath...  76.4 us
    all_to_all x2, blocking collectives, summed_on_arrival(): pieces = lax.all_to_all(cut_along(x, dim, devices), axis, 0, 0, tiled=True)  30 us
    pallas_call x1, Pallas kernels, attended(): pl.pallas_call(functools.partial(attention_kernel, tiles, tile), name='st...  26.8 us
    all_to_all x1, blocking collectives, copy_for_each(): return lax.all_to_all(copies, axis, split_axis=0, concat_axis=0, tiled=True)  14.4 us
    dot_general x1, matrix products, body(): jnp.dot(hidden, down_whole, preferred_element_type=jnp.float32)  7.93 us
    dot_general x1, matrix products, body(): jnp.dot(channel_input, gate_whole, preferred_element_type=jnp.float32)  5.03 us
  transfers between devices with their start and end apart: 1, of which 0 were waited for; matrix products, arithmetic and copies ran while one was open for 3% of the time, Pallas kernels for 57%

profile of v1, /device:TPU:248, one launch (start us, length us, event | category | flops | bytes accessed | tf_op | source)
XLA Modules:
  0.0 182.5 jit_solution(25188713199003989)
XLA Ops:
  6.5 1.8 pad_maximum_fusion
  8.3 0.0 all-gather.2.cloned.1.call-update
  8.4 0.8 copy.16
  9.2 0.8 copy.17
  10.0 0.8 copy.15
  10.9 1.1 concatenate.6.x_ref
  12.0 76.4 %gather_rows.1.kv_ref = bf16[12288,640]{1,0:T(8,128)(2,1)S(1)} custom-call(bf16[192,640]{1,0:T(8,128)(2,1)S(1)} %concatenate.6.x_ref), custom_call_target="tpu_custom_call" | custom-call | flops 10000000000 | bytes 10000000 | tf_op jit(solution)/shard_map/gather_rows/pallas_call | solution.py:186
  88.5 26.8 %stick_attention.1 = (bf16[192,256]{1,0:T(8,128)(2,1)S(1)}, bf16[192,128]{1,0:T(8,128)(2,1)S(1)}) custom-call(s32[1]{0:T(128)} %bitcast.anchor_ref, bf16[192,256]{1,0:T(8,128)(2,1)S(1)} %copy-done.1, bf16[192,128]{1,0:T(8,128)(2,1)S(1)} %pad.4.qb_ref, bf16[12288,640]{1,0:T(8,128)(2,1)S(1)} %gather_rows.1.kv_ref), custom_call_target="tpu_custom_call" | custom-call | flops 7247757312 | bytes 15728640 | tf_op jit(solution)/shard_map/stick_attention/pallas_call | solution.py:282
  115.3 0.4 fusion.30
  115.7 0.5 copy-done.3
  116.2 0.4 fusion.15
  116.6 16.8 %all_to_all.15 = bf16[4,48,2048]{2,1,0:T(8,128)(2,1)S(1)} all-to-all(bf16[4,48,2048]{2,1,0:T(8,128)(2,1)S(1)} %bitcast.10), channel_id=1, replica_groups=mesh['sp'=64,'tp'=4] {'tp'}, dimensions={0} | all-to-all | bytes 1572864 | tf_op jit(solution)/shard_map/all_to_all | solution.py:31
  133.4 0.1 convert_reduce_fusion.1
  133.6 0.1 multiply_reduce_fusion
  133.7 0.3 fusion.24
  134.0 0.1 copy-done.5
  134.1 0.1 fusion.26
  134.2 0.1 broadcast_in_dim.5
  134.3 14.4 %all_to_all.16 = bf16[4,48,2048]{2,1,0:T(8,128)(2,1)S(1)} all-to-all(bf16[4,48,2048]{2,1,0:T(8,128)(2,1)S(1)} %broadcast_in_dim.5), channel_id=1, replica_groups=mesh['sp'=64,'tp'=4] {'tp'}, dimensions={0} | all-to-all | bytes 1572864 | tf_op jit(solution)/shard_map/all_to_all | solution.py:54
  148.7 5.0 %fusion.4 = f32[192,1408]{1,0:T(8,128)} fusion(bf16[192,2048]{1,0:T(8,128)(2,1)S(1)} %bitcast.11, bf16[2048,4224]{1,0:T(8,128)(2,1)} %all-gather.2.cloned.1.call-done), kind=kOutput, calls=%fused_computation.4 | convolution fusion | flops 1107296256 | bytes 7634944 | tf_op jit(solution)/shard_map/dot_general | solution.py:364
  153.7 7.9 %fusion.12 = bf16[192,2048]{1,0:T(8,128)(2,1)S(1)} fusion(bf16[2048,4224]{1,0:T(8,128)(2,1)} %all-gather.2.cloned.1.call-done, bf16[192,2048]{1,0:T(8,128)(2,1)S(1)} %bitcast.12, f32[192,1408]{1,0:T(8,128)} %fusion.4), kind=kOutput, calls=%fused_computation.9 | convolution fusion | flops 2216607744 | bytes 14188544 | tf_op jit(solution)/shard_map/dot_general | solution.py:368
  161.6 13.2 %all_to_all.17 = bf16[4,48,2048]{2,1,0:T(8,128)(2,1)S(1)} all-to-all(bf16[4,48,2048]{2,1,0:T(8,128)(2,1)S(1)} %bitcast.13), channel_id=1, replica_groups=mesh['sp'=64,'tp'=4] {'tp'}, dimensions={0} | all-to-all | bytes 1572864 | tf_op jit(solution)/shard_map/all_to_all | solution.py:31
  174.9 0.1 convert_reduce_fusion
  175.0 0.7 fusion.27
  (16 shorter events, 0.1 us)
Async XLA Ops:
  6.5 108.7 %copy-start = (bf16[256,2048]{1,0:T(8,128)(2,1)S(1)}, bf16[256,2048]{1,0:T(8,128)(2,1)}, u32[]{:S(2)}) copy-start(bf16[256,2048]{1,0:T(8,128)(2,1)} %param.21) | copy-start | bytes 3145732
  6.5 142.1 %all-gather.2.cloned.1.call-start = ((), (), s32[]{:S(2)}) async-start(), calls=%async_computation.3 | async-start | bytes 17571840 | tf_op jit(solution)/shard_map/all_gather | solution.py:38
  12.0 76.5 %copy-start.1 = (bf16[192,256]{1,0:T(8,128)(2,1)S(1)}, bf16[192,256]{1,0:T(8,128)(2,1)}, u32[]{:S(2)}) copy-start(bf16[192,256]{1,0:T(8,128)(2,1)} %qa_ref.1) | copy-start | bytes 294916
  115.3 0.9 copy-start.3
  116.6 17.1 %copy-start.2 = (bf16[48,2048]{1,0:T(8,128)(2,1)S(1)}, bf16[48,2048]{1,0:T(8,128)(2,1)}, u32[]{:S(2)}) copy-start(bf16[48,2048]{1,0:T(8,128)(2,1)} %param.14) | copy-start | bytes 589828
  116.6 17.1 %copy-start.4 = (f32[2048]{0:T(1024)S(1)}, f32[2048]{0:T(1024)}, u32[]{:S(2)}) copy-start(f32[2048]{0:T(1024)} %param.23) | copy-start | bytes 24580
  133.4 0.7 copy-start.5
Sparse Core Ops, SparseCore 0:
  10.1 107.8 all-gather.1
